TPU v7x, 512 devices: a whole 4x8x8 slice. The times are simulated.
512 devices in a mesh: fs: 128 (over z, y, core), tp: 4 (over x).
Axes of the slice: x: 4, y: 8, z: 8, core: 2. Of those that a mesh axis runs over, the one named last changes fastest.
Arguments:
- tokens: bfloat16 [8192, 2048], P('fs', 'tp'), may hold values from -6 to 6
- norm_gain: float32 [2048], P('fs'), may hold values from 0.1 to 1.9
- gate_weight: float32 [128, 2048, 512], P(None, 'fs', 'tp'), may hold values from -0.125 to 0.125
- up_weight: float32 [128, 2048, 512], P(None, 'fs', 'tp'), may hold values from -0.125 to 0.125
- down_weight: float32 [128, 2048, 512], P(None, 'fs', 'tp'), may hold values from -0.25 to 0.25
- route_ids: int32 [8192, 2], P('fs'), may hold values from 0 to 127, all different within a row; in each aligned block of 64 rows (0 to 63, 64 to 127, ...) at most 2 rows name the same one
- group_weight: float32 [8192], P('fs'), may hold values from 0.3 to 1
- logit_gap: float32 [8192], P('fs'), may hold values from -6 to 6
Outputs:
- gate_new: bfloat16 [128, 2048, 512], P('fs', None, 'tp')
- up_new: bfloat16 [128, 2048, 512], P('fs', None, 'tp')
- down_new: bfloat16 [128, 2048, 512], P('fs', None, 'tp')
- mixed: bfloat16 [8192, 2048], P('fs', 'tp')
Inputs may be any that keep to these rules, and one draw needn't show every extreme that they name: `route_ids`: each row names two different experts. In the rows of one device no expert is named by more than 2 rows, a bound that some block reaches.
All inputs are finite; a program needn't handle non-finite values.
Results may differ from a plain program's by a relative error of at most 0.011.
Values may be sent and summed in bfloat16 or wider, within the bound.
A program may use at most 64 MiB of HBM per device.

v0:
```python
import jax
import jax.numpy as jnp
from jax import lax
from jax.sharding import PartitionSpec as P


def in_one_piece(arrays, axis, split_dim, concat_dim, along):
    both = jnp.concatenate(arrays, axis=along)
    out, at, finished = (
        lax.all_to_all(both, axis, split_axis=split_dim, concat_axis=concat_dim, tiled=True),
        0,
        [],
    )
    for a in arrays:
        finished.append(lax.slice_in_dim(out, at, at + a.shape[along], axis=along))
        at += a.shape[along]
    return tuple(finished)


def cut_along(shard, dim, size):
    lengths = shard.shape
    parts = shard.reshape(*lengths[:dim], size, lengths[dim] // size, *lengths[dim + 1 :])
    return jnp.moveaxis(parts, dim, 0)


def summed_on_arrival(shard, axis, dim):
    size = lax.axis_size(axis)
    parts = lax.all_to_all(cut_along(shard, dim, size), axis, 0, 0, tiled=True)
    return jnp.sum(parts.astype(jnp.float32), axis=0)


def slot_tables(route_ids, experts, capacity):
    row_count = route_ids.shape[0]
    pair_count = 2 * row_count
    flat_ids = route_ids.reshape(pair_count)
    onehot = (flat_ids[:, None] == jnp.arange(experts, dtype=jnp.int32)[None, :]).astype(
        jnp.bfloat16
    )
    positions = jnp.arange(pair_count, dtype=jnp.int32)
    below_mask = (positions[:, None] > positions[None, :]).astype(jnp.bfloat16)
    before = jnp.dot(below_mask, onehot, preferred_element_type=jnp.float32)
    ranked = jnp.sum(before * onehot.astype(jnp.float32), axis=1).astype(jnp.int32)
    return (flat_ids * capacity + ranked).reshape(row_count, 2)


def first_products(slot_rows, gate_cols, up_cols):
    shard_cols = lax.all_gather(slot_rows, "tp", axis=1, tiled=True)
    return (
        jnp.dot(shard_cols, gate_cols, preferred_element_type=jnp.float32),
        jnp.dot(shard_cols, up_cols, preferred_element_type=jnp.float32),
    )


def body(
    tokens, norm_gain, gate_weight, up_weight, down_weight, route_ids, group_weight, logit_gap
):
    experts = gate_weight.shape[0]
    tok_rows = tokens.shape[0]
    capacity = max(2, (3 * tok_rows + experts - 1) // experts)
    folded = norm_gain[None, :, None]
    gate_local = (gate_weight * folded).astype(jnp.bfloat16)
    up_local = (up_weight * folded).astype(jnp.bfloat16)
    down_local = down_weight.astype(jnp.bfloat16)
    slot_ids = slot_tables(route_ids, experts, capacity)
    slot_range = jnp.arange(experts * capacity, dtype=jnp.int32)
    matches = (slot_ids[None, :, :] == slot_range[:, None, None]).astype(jnp.int32)
    dispatch = jnp.sum(matches, axis=2).astype(jnp.bfloat16)
    outgoing = jnp.dot(dispatch, tokens, preferred_element_type=jnp.float32).astype(jnp.bfloat16)
    outgoing = outgoing.reshape(experts, capacity, tokens.shape[1])
    arrived = lax.all_to_all(outgoing, "fs", split_axis=0, concat_axis=0, tiled=True)
    slot_rows = arrived.reshape(experts * capacity, tokens.shape[1])
    gate_out, up_out, down_out = in_one_piece((gate_local, up_local, down_local), "fs", 0, 1, 2)
    gate_acc, up_acc = first_products(slot_rows, gate_out[0], up_out[0])
    hidden = (jax.nn.silu(gate_acc) * up_acc).astype(jnp.bfloat16)
    partial_value = lax.dot_general(
        hidden, down_out[0], (((1,), (1,)), ((), ())), preferred_element_type=jnp.float32
    )
    summed = summed_on_arrival(partial_value.astype(jnp.bfloat16), "tp", 1).astype(jnp.bfloat16)
    returned = lax.all_to_all(
        summed.reshape(experts, capacity, summed.shape[1]),
        "fs",
        split_axis=0,
        concat_axis=0,
        tiled=True,
    )
    back_rows = returned.reshape(experts * capacity, summed.shape[1])
    pick_first = (slot_ids[:, 0:1] == slot_range[None, :]).astype(jnp.bfloat16)
    pick_second = (slot_ids[:, 1:2] == slot_range[None, :]).astype(jnp.bfloat16)
    first_vals = jnp.dot(pick_first, back_rows, preferred_element_type=jnp.float32)
    second_vals = jnp.dot(pick_second, back_rows, preferred_element_type=jnp.float32)
    first_weight = group_weight * jax.nn.sigmoid(logit_gap)
    second_weight = group_weight * jax.nn.sigmoid(-logit_gap)
    mixed = (first_weight[:, None] * first_vals + second_weight[:, None] * second_vals).astype(
        jnp.bfloat16
    )
    return (gate_out, up_out, down_out, mixed)


def solution(mesh):
    return jax.shard_map(
        body,
        mesh=mesh,
        in_specs=(
            P("fs", "tp"),
            P("fs"),
            P(None, "fs", "tp"),
            P(None, "fs", "tp"),
            P(None, "fs", "tp"),
            P("fs", None),
            P("fs"),
            P("fs"),
        ),
        out_specs=(P("fs", None, "tp"), P("fs", None, "tp"), P("fs", None, "tp"), P("fs", "tp")),
        check_vma=False,
    )
```

profile of v0, /device:TPU:1, one launch (start us, length us, event | category | flops | bytes accessed | tf_op | source)
XLA Modules:
  0.0 146.3 jit_solution(3357822212724454041)
XLA Ops:
  7.2 0.0 copy-start
  7.2 0.0 copy-start.4
  7.2 0.9 copy.27
  8.1 0.1 eq.56
  8.2 0.2 fusion.3
  8.4 0.0 copy-start.5
  8.4 0.0 copy-start.6
  8.4 0.0 copy-start.9
  8.4 0.1 convert_element_type.53
  8.6 0.1 copy.28
  8.6 0.8 multiply_add_fusion
  9.5 0.1 convert_reduce_fusion
  9.5 0.0 copy-done
  9.6 0.2 convolution_convert_fusion.1
  9.8 0.8 reshape.41
  10.6 18.4 %all-to-all-start.1 = ((bf16[128,2,512]{2,1,0:T(2,128)(2,1)}), bf16[128,2,512]{2,1,0:T(2,128)(2,1)S(1)}, u32[]{:S(2)}, u32[]{:S(2)}) async-start(bf16[128,2,512]{2,1,0:T(2,128)(2,1)} %reshape.41), calls=%async_computation.1 | async-start | bytes 524288 | tf_op jit(solution)/shard_map/all_to_all | solution.py:70
  29.0 0.0 copy-done.4
  29.0 0.1 convert_element_type.49
  29.1 0.0 copy-done.5
  29.1 0.0 copy-done.6
  29.1 0.0 copy-done.9
  29.2 0.2 multiply_convert_fusion.1
  29.4 1.4 pad_maximum_fusion
  30.8 13.5 %all-to-all-done.1 = bf16[128,2,512]{2,1,0:T(2,128)(2,1)S(1)} async-done(((bf16[128,2,512]{2,1,0:T(2,128)(2,1)}), bf16[128,2,512]{2,1,0:T(2,128)(2,1)S(1)}, u32[]{:S(2)}, u32[]{:S(2)}) %all-to-all-start.1) | async-done | bytes 262176 | tf_op jit(solution)/shard_map/all_to_all | solution.py:70
  44.3 5.6 %all-to-all-start = ((bf16[128,16,384]{2,1,0:T(8,128)(2,1)}), bf16[128,16,384]{2,1,0:T(8,128)(2,1)S(1)}, u32[]{:S(2)}, u32[]{:S(2)}) async-start(bf16[128,16,384]{2,1,0:T(8,128)(2,1)} %pad_maximum_fusion), calls=%async_computation | async-start | bytes 3145728 | tf_op jit(solution)/shard_map/all_to_all | solution.py:10
  49.8 0.0 all-gather.2.cloned.1.call-start
  49.9 0.8 reshape.42
  50.7 0.0 all-gather.2.cloned.1.call-update
  50.7 40.4 %all-to-all-done = bf16[128,16,384]{2,1,0:T(8,128)(2,1)S(1)} async-done(((bf16[128,16,384]{2,1,0:T(8,128)(2,1)}), bf16[128,16,384]{2,1,0:T(8,128)(2,1)S(1)}, u32[]{:S(2)}, u32[]{:S(2)}) %all-to-all-start) | async-done | bytes 1572896 | tf_op jit(solution)/shard_map/all_to_all | solution.py:10
  91.2 1.1 fusion.21
  92.2 0.0 copy-start.2
  92.2 0.0 copy-start.3
  92.2 2.2 %fusion.7 = f32[256,128]{1,0:T(8,128)S(1)} fusion(bf16[256,2048]{1,0:T(8,128)(2,1)} %all-gather.2.cloned.1.call-done, bf16[1,2048,128]{2,1,0:T(8,128)(2,1)} %get-tuple-element.6), kind=kOutput, calls=%fused_computation.16 | convolution fusion | flops 134217728 | bytes 1703936 | tf_op jit(solution)/shard_map/dot_general | solution.py:49
  94.4 0.0 copy-done.1
  94.4 0.8 convolution_convert_fusion
  95.2 0.0 copy-done.2
  95.2 0.0 copy-done.3
  95.2 0.1 copy.32
  95.3 18.0 %all_to_all.27 = bf16[4,256,512]{2,1,0:T(8,128)(2,1)S(1)} all-to-all(bf16[4,256,512]{2,1,0:T(8,128)(2,1)S(1)} %bitcast.29), channel_id=1, replica_groups=mesh['fs'=128,'tp'=4] {'tp'}, dimensions={0} | all-to-all | bytes 2097152 | tf_op jit(solution)/shard_map/all_to_all | solution.py:28
  113.3 0.2 reduce_sum.32
  113.6 0.8 reshape.44
  114.4 8.7 %all-to-all-start.3 = ((bf16[128,2,512]{2,1,0:T(2,128)(2,1)}), bf16[128,2,512]{2,1,0:T(2,128)(2,1)S(1)}, u32[]{:S(2)}, u32[]{:S(2)}) async-start(bf16[128,2,512]{2,1,0:T(2,128)(2,1)} %reshape.44), calls=%async_computation.3 | async-start | bytes 524288 | tf_op jit(solution)/shard_map/all_to_all | solution.py:79
  123.1 0.0 copy-done.7
  123.1 0.0 copy-done.8
  123.1 15.2 %all-to-all-done.3 = bf16[128,2,512]{2,1,0:T(2,128)(2,1)S(1)} async-done(((bf16[128,2,512]{2,1,0:T(2,128)(2,1)}), bf16[128,2,512]{2,1,0:T(2,128)(2,1)S(1)}, u32[]{:S(2)}, u32[]{:S(2)}) %all-to-all-start.3) | async-done | bytes 262176 | tf_op jit(solution)/shard_map/all_to_all | solution.py:79
  138.3 0.1 reshape.45
  138.4 0.2 convolution_multiply_fusion.1
  138.6 0.8 fusion.2
  (7 shorter events, 0.0 us)
Async XLA Ops:
  7.2 2.4 %copy-start = (bf16[64,512]{1,0:T(8,128)(2,1)S(1)}, bf16[64,512]{1,0:T(8,128)(2,1)}, u32[]{:S(2)}) copy-start(bf16[64,512]{1,0:T(8,128)(2,1)} %param.8) | copy-start | bytes 196612
  7.2 21.9 %copy-start.4 = (f32[128,16,128]{2,1,0:T(8,128)S(1)}, f32[128,16,128]{2,1,0:T(8,128)}, u32[]{:S(2)}) copy-start(f32[128,16,128]{2,1,0:T(8,128)} %param.12) | copy-start | bytes 3145732
  8.4 20.7 %copy-start.5 = (f32[128,16,128]{2,1,0:T(8,128)S(1)}, f32[128,16,128]{2,1,0:T(8,128)}, u32[]{:S(2)}) copy-start(f32[128,16,128]{2,1,0:T(8,128)} %param.10) | copy-start | bytes 3145732
  8.4 20.7 %copy-start.6 = (f32[128,16,128]{2,1,0:T(8,128)S(1)}, f32[128,16,128]{2,1,0:T(8,128)}, u32[]{:S(2)}) copy-start(f32[128,16,128]{2,1,0:T(8,128)} %param.11) | copy-start | bytes 3145732
  8.4 20.7 %copy-start.9 = (f32[16]{0:T(128)S(1)}, f32[16]{0:T(128)}, u32[]{:S(2)}) copy-start(f32[16]{0:T(128)} %param.9) | copy-start | bytes 196
  10.6 33.6 %all-to-all-start.1 = ((bf16[128,2,512]{2,1,0:T(2,128)(2,1)}), bf16[128,2,512]{2,1,0:T(2,128)(2,1)S(1)}, u32[]{:S(2)}, u32[]{:S(2)}) async-start(bf16[128,2,512]{2,1,0:T(2,128)(2,1)} %reshape.41), calls=%async_computation.1 | async-start | bytes 524288 | tf_op jit(solution)/shard_map/all_to_all | solution.py:70
  44.3 46.9 %all-to-all-start = ((bf16[128,16,384]{2,1,0:T(8,128)(2,1)}), bf16[128,16,384]{2,1,0:T(8,128)(2,1)S(1)}, u32[]{:S(2)}, u32[]{:S(2)}) async-start(bf16[128,16,384]{2,1,0:T(8,128)(2,1)} %pad_maximum_fusion), calls=%async_computation | async-start | bytes 3145728 | tf_op jit(solution)/shard_map/all_to_all | solution.py:10
  49.8 42.4 %all-gather.2.cloned.1.call-start = ((), (), s32[]{:S(2)}) async-start(), calls=%async_computation.4 | async-start | bytes 1310720 | tf_op jit(solution)/shard_map/all_gather | solution.py:47
  92.2 3.0 %copy-start.2 = (bf16[1,2048,128]{2,1,0:T(8,128)(2,1)}, bf16[1,2048,128]{2,1,0:T(8,128)(2,1)S(1)}, u32[]{:S(2)}) copy-start(bf16[1,2048,128]{2,1,0:T(8,128)(2,1)S(1)} %get-tuple-element.4) | copy-start | bytes 1572868
  92.2 3.0 %copy-start.3 = (bf16[1,2048,128]{2,1,0:T(8,128)(2,1)}, bf16[1,2048,128]{2,1,0:T(8,128)(2,1)S(1)}, u32[]{:S(2)}) copy-start(bf16[1,2048,128]{2,1,0:T(8,128)(2,1)S(1)} %get-tuple-element.5) | copy-start | bytes 1572868
  92.2 2.2 %copy-start.1 = (bf16[256,2048]{1,0:T(8,128)(2,1)S(1)}, bf16[256,2048]{1,0:T(8,128)(2,1)}, u32[]{:S(2)}) copy-start(bf16[256,2048]{1,0:T(8,128)(2,1)} %all-gather.2.cloned.1.call-done) | copy-start | bytes 3145732
  113.3 9.8 %copy-start.7 = (f32[64]{0:T(128)S(1)}, f32[64]{0:T(128)}, u32[]{:S(2)}) copy-start(f32[64]{0:T(128)} %param.14) | copy-start | bytes 772
  113.3 9.8 %copy-start.8 = (f32[64]{0:T(128)S(1)}, f32[64]{0:T(128)}, u32[]{:S(2)}) copy-start(f32[64]{0:T(128)} %param.15) | copy-start | bytes 772
  114.4 23.9 %all-to-all-start.3 = ((bf16[128,2,512]{2,1,0:T(2,128)(2,1)}), bf16[128,2,512]{2,1,0:T(2,128)(2,1)S(1)}, u32[]{:S(2)}, u32[]{:S(2)}) async-start(bf16[128,2,512]{2,1,0:T(2,128)(2,1)} %reshape.44), calls=%async_computation.3 | async-start | bytes 524288 | tf_op jit(solution)/shard_map/all_to_all | solution.py:79
Sparse Core Ops, SparseCore 0:
  52.8 28.4 all-gather.1
where the time goes:
time: 147 us; the launch traced here: 146 us
  waiting for transfers between devices  69.1 us (47%)
  starting transfers between devices  32.7 us (22%)
  blocking collectives  18 us (12%)
  between operations  14.3 us (10%)
  local copies, waits for them, and re-layouts  4.93 us (3%)
  matrix products  4.44 us (3%)
  other arithmetic  2.85 us (2%)
    all_to_all x1, waiting for transfers between devices, in_one_piece(): lax.all_to_all(both, axis, split_axis=split_dim, concat_axis=concat_dim,...  40.4 us
    all_to_all x1, starting transfers between devices, body(): lax.all_to_all(outgoing, 'fs', split_axis=0, concat_axis=0, tiled=True)  18.4 us
    all_to_all x1, blocking collectives, summed_on_arrival(): parts = lax.all_to_all(cut_along(shard, dim, size), axis, 0, 0, tiled=True)  18 us
    all_to_all x1, waiting for transfers between devices, body(): lax.all_to_all(summed.reshape(experts, capacity, summed.shape[1]), 'fs',...  15.2 us
    all_to_all x1, waiting for transfers between devices, body(): lax.all_to_all(outgoing, 'fs', split_axis=0, concat_axis=0, tiled=True)  13.5 us
    all_to_all x1, starting transfers between devices, body(): lax.all_to_all(summed.reshape(experts, capacity, summed.shape[1]), 'fs',...  8.7 us
    all_to_all x1, starting transfers between devices, in_one_piece(): lax.all_to_all(both, axis, split_axis=split_dim, concat_axis=concat_dim,...  5.57 us
  transfers between devices with their start and end apart: 4, of which 3 were waited for; matrix products, arithmetic and copies ran while one was open for 2% of the time, Pallas kernels for 0%

commit v1 on v0

v1 whole, which is shorter than its diff:
```python
import functools

import jax
import jax.numpy as jnp
from jax import lax
from jax.experimental import pallas as pl
from jax.experimental.pallas import tpu as pltpu
from jax.sharding import PartitionSpec as P

MESH = pl.DeviceIdType.MESH
F32, BF16 = jnp.float32, jnp.bfloat16
STRIDE = 45


def partner(me, off):
    z, y, c = me // 16, (me // 2) % 8, me % 2
    dz, dy, dc = off // 16, (off // 2) % 8, off % 2
    return ((z + dz) % 8) * 16 + ((y + dy) % 8) * 2 + (c + dc) % 2


def each_partner(me, n_fs, step):
    def turn(i, off):
        step(partner(me, off))
        later = off + STRIDE
        return jnp.where(later >= n_fs, later - (n_fs - 1), later)

    lax.fori_loop(0, n_fs - 1, turn, jnp.int32(1))


def kernel(
    n_fs, n_tp,
    ids_ref, group_ref, gap_ref, gain_ref, tokens_ref, gate_ref, up_ref, down_ref,
    gate_in, up_in, down_in, mixed_ref,
    ids, group, gap, gain, tokens, gate_f, up_f, down_f,
    gate_out, up_out, down_out, tok_out, tok_in, ret_out, ret_in,
    rows_all, hid_all, down_q, wide, picks,
    local_sem, send_sem, recv_sem,
):
    me, j = lax.axis_index("fs"), lax.axis_index("tp")
    slots = 2 * n_fs
    barrier = pltpu.get_barrier_semaphore()

    def greet(d):
        pl.semaphore_signal(barrier, inc=1, device_id={"fs": d}, device_id_type=MESH)

    each_partner(me, n_fs, greet)
    for k in range(1, n_tp):
        pl.semaphore_signal(
            barrier, inc=1, device_id={"tp": (j + k) % n_tp}, device_id_type=MESH
        )

    small = [(ids_ref, ids), (group_ref, group), (gap_ref, gap), (gain_ref, gain), (tokens_ref, tokens)]
    large = [(down_ref, down_f), (gate_ref, gate_f), (up_ref, up_f)]
    loads = [
        pltpu.make_async_copy(src, dst, local_sem.at[i])
        for i, (src, dst) in enumerate(small + large)
    ]
    for c in loads:
        c.start()
    for c in loads[:5]:
        c.wait()

    count = tokens.shape[0]
    slot = lax.broadcasted_iota(jnp.int32, (slots, count), 0)
    first = (slot // 2 == ids[0:1, :]).astype(F32)
    second = (slot // 2 == ids[1:2, :]).astype(F32)
    earlier = (
        lax.broadcasted_iota(jnp.int32, (count, count), 0)
        < lax.broadcasted_iota(jnp.int32, (count, count), 1)
    ).astype(BF16)
    before = jnp.dot((first + second).astype(BF16), earlier, preferred_element_type=F32)
    ranked = (before == (slot % 2).astype(F32)).astype(F32)
    first, second = first * ranked, second * ranked
    picks[0] = first.astype(BF16)
    picks[1] = second.astype(BF16)
    outgoing = jnp.dot((first + second).astype(BF16), tokens[...], preferred_element_type=F32)
    for b in range(4):
        wide[pl.ds(b, slots, stride=4), :] = outgoing[:, b * 128 : (b + 1) * 128]
    tok_out[...] = wide[...].astype(BF16).reshape(n_fs, 8, 128)

    diagonal = lax.broadcasted_iota(jnp.int32, (16, 16), 0) == lax.broadcasted_iota(
        jnp.int32, (16, 16), 1
    )
    scale = jnp.sum(jnp.where(diagonal, gain[...], 0.0), axis=1, keepdims=True)
    scale = jnp.broadcast_to(scale, (16, 128))[None]

    def round_down(i, _):
        at = pl.ds(i * 8, 8)
        down_out[at] = down_f[at].astype(BF16)
        return 0

    def round_first(i, _):
        at = pl.ds(i * 8, 8)
        gate_out[at] = (gate_f[at] * scale).astype(BF16)
        up_out[at] = (up_f[at] * scale).astype(BF16)
        return 0

    loads[5].wait()
    lax.fori_loop(0, n_fs // 8, round_down, 0)
    loads[6].wait()
    loads[7].wait()
    lax.fori_loop(0, n_fs // 8, round_first, 0)

    pl.semaphore_wait(barrier, n_fs - 1 + n_tp - 1)

    def exchange(i, src, dst):
        def send(d):
            pltpu.make_async_remote_copy(
                src_ref=src.at[d], dst_ref=dst.at[me],
                send_sem=send_sem.at[i], recv_sem=recv_sem.at[i],
                device_id={"fs": d}, device_id_type=MESH,
            ).start()

        each_partner(me, n_fs, send)
        dst[me] = src[me]

    def all_of(i, src, dst, copies=n_fs - 1):
        return pltpu.make_async_remote_copy(
            src_ref=src.at[pl.ds(0, copies)], dst_ref=dst.at[pl.ds(0, copies)],
            send_sem=send_sem.at[i], recv_sem=recv_sem.at[i],
            device_id={"tp": (j + 1) % n_tp}, device_id_type=MESH,
        )

    exchange(0, tok_out, tok_in)
    exchange(1, down_out, down_in)
    exchange(2, gate_out, gate_in)
    exchange(3, up_out, up_in)

    def across(i, src_of, dst):
        for k in range(1, n_tp):
            to = (j + k) % n_tp
            pltpu.make_async_remote_copy(
                src_ref=src_of(to), dst_ref=dst.at[j],
                send_sem=send_sem.at[i], recv_sem=recv_sem.at[i],
                device_id={"tp": to}, device_id_type=MESH,
            ).start()

    all_of(0, tok_out, tok_in).wait_recv()
    wide[...] = tok_in[...].reshape(slots * 4, 128).astype(F32)
    for b in range(4):
        rows_all[j, :, b * 128 : (b + 1) * 128] = wide[pl.ds(b, slots, stride=4), :].astype(BF16)
    across(4, lambda to: rows_all.at[j], rows_all)

    all_of(1, down_out, down_in).wait_recv()
    across(5, lambda to: down_in.at[pl.ds(to * (n_fs // n_tp), n_fs // n_tp)], down_q)
    down_q[j] = down_in[pl.ds(j * (n_fs // n_tp), n_fs // n_tp)]

    all_of(4, rows_all, rows_all, n_tp - 1).wait_recv()
    all_of(2, gate_out, gate_in).wait_recv()
    depth = n_fs // n_tp

    def product(w):
        total = None
        for k in range(n_tp):
            block = w[k * depth : (k + 1) * depth].reshape(depth * 16, 128)
            term = jnp.dot(rows_all[k], block, preferred_element_type=F32)
            total = term if total is None else total + term
        return total

    gate_acc = product(gate_in)
    all_of(3, up_out, up_in).wait_recv()
    up_acc = product(up_in)
    hid_all[j] = (gate_acc / (1.0 + jnp.exp(-gate_acc)) * up_acc).astype(BF16)
    across(6, lambda to: hid_all.at[j], hid_all)
    all_of(5, down_q, down_q, n_tp - 1).wait_recv()
    all_of(6, hid_all, hid_all, n_tp - 1).wait_recv()
    total = None
    for k in range(n_tp):
        term = lax.dot_general(
            hid_all[k], down_q[k].reshape(depth * 16, 128), (((1,), (1,)), ((), ())),
            preferred_element_type=F32,
        )
        total = term if total is None else total + term
    for b in range(4):
        wide[pl.ds(b, slots, stride=4), :] = total[:, b * 128 : (b + 1) * 128]
    ret_out[...] = wide[...].astype(BF16).reshape(n_fs, 8, 128)
    exchange(7, ret_out, ret_in)

    here = lax.broadcasted_iota(jnp.int32, (count, count), 0) == lax.broadcasted_iota(
        jnp.int32, (count, count), 1
    )
    w_first = group[...] * jax.nn.sigmoid(gap[...])
    w_second = group[...] * jax.nn.sigmoid(-gap[...])
    w_first = jnp.sum(jnp.where(here, w_first, 0.0), axis=1, keepdims=True)
    w_second = jnp.sum(jnp.where(here, w_second, 0.0), axis=1, keepdims=True)

    all_of(7, ret_out, ret_in).wait_recv()
    wide[...] = ret_in[...].reshape(slots * 4, 128).astype(F32)
    for b in range(4):
        block = wide[pl.ds(b, slots, stride=4), :].astype(BF16)
        value = [
            lax.dot_general(
                picks[k], block, (((0,), (0,)), ((), ())), preferred_element_type=F32
            )
            for k in range(2)
        ]
        mixed_ref[:, b * 128 : (b + 1) * 128] = (
            w_first * value[0] + w_second * value[1]
        ).astype(BF16)

    for i, (src, dst) in enumerate(
        [(tok_out, tok_in), (down_out, down_in), (gate_out, gate_in), (up_out, up_in)]
    ):
        all_of(i, src, dst).wait_send()
    for i, a in ((4, rows_all), (5, down_q), (6, hid_all)):
        all_of(i, a, a, n_tp - 1).wait_send()
    all_of(7, ret_out, ret_in).wait_send()


def body(
    tokens, norm_gain, gate_weight, up_weight, down_weight, route_ids, group_weight, logit_gap
):
    n_fs, n_tp = lax.axis_size("fs"), lax.axis_size("tp")
    count, width = tokens.shape
    experts, depth, units = gate_weight.shape
    whole = pl.BlockSpec(memory_space=pltpu.VMEM)
    anywhere = pl.BlockSpec(memory_space=pl.ANY)
    weights = jax.ShapeDtypeStruct((experts, depth, units), BF16)
    slots = 2 * n_fs
    gate_new, up_new, down_new, mixed = pl.pallas_call(
        functools.partial(kernel, n_fs, n_tp),
        out_shape=(weights, weights, weights, jax.ShapeDtypeStruct((count, width), BF16)),
        in_specs=[anywhere] * 8,
        out_specs=[whole] * 4,
        scratch_shapes=[
            pltpu.VMEM((2, count), jnp.int32),
            pltpu.VMEM((1, count), F32),
            pltpu.VMEM((1, count), F32),
            pltpu.VMEM((1, depth), F32),
            pltpu.VMEM((count, width), BF16),
        ]
        + [pltpu.VMEM((experts, depth, units), F32)] * 3
        + [pltpu.VMEM((experts, depth, units), BF16)] * 3
        + [pltpu.VMEM((n_fs, 8, 128), BF16)] * 4
        + [
            pltpu.VMEM((n_tp, slots, width), BF16),
            pltpu.VMEM((n_tp, slots, units), BF16),
            pltpu.VMEM((n_tp, n_fs // n_tp, depth, units), BF16),
            pltpu.VMEM((slots * 4, 128), F32),
            pltpu.VMEM((2, slots, count), BF16),
            pltpu.SemaphoreType.DMA((8,)),
            pltpu.SemaphoreType.DMA((8,)),
            pltpu.SemaphoreType.DMA((8,)),
        ],
        compiler_params=pltpu.CompilerParams(
            collective_id=0, has_side_effects=True, vmem_limit_bytes=40 * 1024 * 1024
        ),
    )(
        route_ids.T, group_weight.reshape(1, count), logit_gap.reshape(1, count),
        norm_gain.reshape(1, depth), tokens, gate_weight, up_weight, down_weight,
    )
    shape = (1, experts * depth, units)
    return gate_new.reshape(shape), up_new.reshape(shape), down_new.reshape(shape), mixed


def solution(mesh):
    return jax.shard_map(
        body,
        mesh=mesh,
        in_specs=(
            P("fs", "tp"), P("fs"), P(None, "fs", "tp"), P(None, "fs", "tp"),
            P(None, "fs", "tp"), P("fs", None), P("fs"), P("fs"),
        ),
        out_specs=(P("fs", None, "tp"), P("fs", None, "tp"), P("fs", None, "tp"), P("fs", "tp")),
        check_vma=False,
    )
```

time: 147 us -> 93.5 us (0.64)
  Pallas kernels: 0 us -> 84.3 us
  waiting for transfers between devices: 69.1 us -> 0 us
  starting transfers between devices: 32.7 us -> 0 us
  blocking collectives: 18 us -> 0 us
  between operations: 14.3 us -> 0.68 us
  matrix products: 4.44 us -> 0 us
  local copies, waits for them, and re-layouts: 4.93 us -> 8.2 us
  other arithmetic: 2.85 us -> 0 us
    pallas_call x0 -> x1, Pallas kernels: none -> 84.3 us  [body(): pl.pallas_call(functools.partial(kernel, n_fs, n_tp), out_shape=(weights,...]
    all_to_all x3 -> x0, waiting for transfers between devices: 69.1 us -> none  [the longest x1 40.4 us: in_one_piece(): lax.all_to_all(both, axis, split_axis=split_dim, concat_axis=concat_dim,...]
    all_to_all x3 -> x0, starting transfers between devices: 32.7 us -> none  [the longest x1 18.4 us: body(): lax.all_to_all(outgoing, 'fs', split_axis=0, concat_axis=0, tiled=True)]
    all_to_all x1 -> x0, blocking collectives: 18 us -> none  [summed_on_arrival(): parts = lax.all_to_all(cut_along(shard, dim, size), axis, 0, 0, tiled=True)]
    unnamed x21 -> x20, local copies, waits for them, and re-layouts: 0.91 us -> 8.2 us
    dot_general x6 -> x0, matrix products: 4.44 us -> none  [the longest x1 2.18 us: first_products(): jnp.dot(shard_cols, gate_cols, preferred_element_type=jnp.float32)]
    reshape x5 -> x0, local copies, waits for them, and re-layouts: 2.61 us -> none  [the longest x1 0.81 us: body(): summed.reshape(experts, capacity, summed.shape[1])]
  transfers between devices with their start and end apart: 4 -> 0, of which waited for: 3 -> 0; matrix products, arithmetic and copies ran while one was open for 2% -> 0% of each run, Pallas kernels for 0% -> 0%
where the time goes in v1:
time: 93.5 us; the launch traced here: 93.2 us
  Pallas kernels  84.3 us (90%)
  local copies, waits for them, and re-layouts  8.2 us (9%)
    pallas_call x1, Pallas kernels, body(): pl.pallas_call(functools.partial(kernel, n_fs, n_tp), out_shape=(weights,...  84.3 us
    unnamed x20, local copies, waits for them, and re-layouts  8.2 us

profile of v1, /device:TPU:1, one launch (start us, length us, event | category | flops | bytes accessed | tf_op | source)
XLA Modules:
  0.0 93.2 jit_solution(18063166260053717228)
XLA Ops:
  0.6 0.0 copy-start.6
  0.6 0.0 copy-start.7
  0.7 0.0 copy-start.4
  0.7 0.0 copy-start.5
  0.7 0.6 copy-done.6
  1.3 0.0 copy-done.7
  1.3 0.0 copy-done.4
  1.3 0.0 copy-done.5
  1.3 0.0 copy-start
  1.4 1.2 %copy-done = f32[128,16,128]{2,1,0:T(8,128)S(1)} copy-done((f32[128,16,128]{2,1,0:T(8,128)S(1)}, f32[128,16,128]{2,1,0:T(8,128)}, u32[]{:S(2)}) %copy-start) | copy-done | bytes 1048600
  2.6 0.0 copy-start.1
  2.6 1.2 %copy-done.1 = f32[128,16,128]{2,1,0:T(8,128)S(1)} copy-done((f32[128,16,128]{2,1,0:T(8,128)S(1)}, f32[128,16,128]{2,1,0:T(8,128)}, u32[]{:S(2)}) %copy-start.1) | copy-done | bytes 1048600
  3.8 0.0 copy-start.2
  3.8 1.2 %copy-done.2 = f32[128,16,128]{2,1,0:T(8,128)S(1)} copy-done((f32[128,16,128]{2,1,0:T(8,128)S(1)}, f32[128,16,128]{2,1,0:T(8,128)}, u32[]{:S(2)}) %copy-start.2) | copy-done | bytes 1048600
  5.0 0.0 copy-start.3
  5.0 0.8 copy-done.3
  5.9 84.3 %shard_map.111 = (bf16[128,16,128]{2,1,0:T(8,128)(2,1)S(1)}, bf16[128,16,128]{2,1,0:T(8,128)(2,1)S(1)}, bf16[128,16,128]{2,1,0:T(8,128)(2,1)S(1)}, bf16[64,512]{1,0:T(8,128)(2,1)S(1)}) custom-call(s32[2,64]{1,0:T(2,128)S(1)} %bitcast.10, f32[1,64]{1,0:T(1,128)S(1)} %bitcast.11, f32[1,64]{1,0:T(1,128)S(1)} %bitcast.12, f32[1,16]{1,0:T(1,128)S(1)} %bitcast.13, ...), custom_call_target="tpu_custom_call" | custom-call | tf_op jit(solution)/shard_map/pallas_call | solution.py:220
  90.2 0.8 copy.16
  91.0 0.8 copy.17
  91.8 0.8 copy.18
  92.6 0.6 copy.19
Async XLA Ops:
  0.6 0.7 copy-start.6
  0.6 0.7 copy-start.7
  0.7 0.7 copy-start.4
  0.7 0.7 copy-start.5
  1.3 1.2 %copy-start = (f32[128,16,128]{2,1,0:T(8,128)S(1)}, f32[128,16,128]{2,1,0:T(8,128)}, u32[]{:S(2)}) copy-start(f32[128,16,128]{2,1,0:T(8,128)} %gate_ref.1) | copy-start | bytes 3145732
  2.6 1.2 %copy-start.1 = (f32[128,16,128]{2,1,0:T(8,128)S(1)}, f32[128,16,128]{2,1,0:T(8,128)}, u32[]{:S(2)}) copy-start(f32[128,16,128]{2,1,0:T(8,128)} %up_ref.1) | copy-start | bytes 3145732
  3.8 1.2 %copy-start.2 = (f32[128,16,128]{2,1,0:T(8,128)S(1)}, f32[128,16,128]{2,1,0:T(8,128)}, u32[]{:S(2)}) copy-start(f32[128,16,128]{2,1,0:T(8,128)} %down_ref.1) | copy-start | bytes 3145732
  5.0 0.8 copy-start.3

commit v2 on v1

--- a/solution.py
+++ b/solution.py
@@ -10,21 +10,60 @@
 MESH = pl.DeviceIdType.MESH
 F32, BF16 = jnp.float32, jnp.bfloat16
 STRIDE = 45
-
-
-def partner(me, off):
+FAR_FIRST = (4, 3, 5, 2, 6, 1, 7, 0)
+
+
+def partner(me, dz, dy, dc):
     z, y, c = me // 16, (me // 2) % 8, me % 2
-    dz, dy, dc = off // 16, (off // 2) % 8, off % 2
     return ((z + dz) % 8) * 16 + ((y + dy) % 8) * 2 + (c + dc) % 2
 
 
 def each_partner(me, n_fs, step):
-    def turn(i, off):
-        step(partner(me, off))
-        later = off + STRIDE
-        return jnp.where(later >= n_fs, later - (n_fs - 1), later)
-
-    lax.fori_loop(0, n_fs - 1, turn, jnp.int32(1))
+    def at(n):
+        off = (n * STRIDE) % n_fs
+        step(partner(me, off // 16, (off // 2) % 8, off % 2))
+
+    def turn(i, _):
+        for u in range(8):
+            at(i * 8 + u)
+        return 0
+
+    for u in range(1, 8):
+        at(u)
+    lax.fori_loop(1, n_fs // 8, turn, 0)
+
+
+def far_partners_first(me, step):
+    def turn(k, _):
+        dz = (4 + (1 - 2 * (k % 2)) * ((k + 1) // 2)) % 8
+        for dy in FAR_FIRST:
+            for dc in range(2):
+                step(partner(me, dz, dy, dc))
+        return 0
+
+    lax.fori_loop(0, 7, turn, 0)
+    for dy in FAR_FIRST:
+        for dc in range(2):
+            if dy or dc:
+                step(partner(me, 0, dy, dc))
+
+
+def each_partner_of_rows(me, low, high, step):
+    z, y, c = me // 16, (me // 2) % 8, me % 2
+
+    def turn(row, _):
+        for dy in FAR_FIRST[:-1]:
+            for dc in range(2):
+                step(row * 16 + ((y + dy) % 8) * 2 + (c + dc) % 2)
+        step(row * 16 + y * 2 + (c + 1) % 2)
+
+        @pl.when(row != z)
+        def _():
+            step(row * 16 + y * 2 + c)
+
+        return 0
+
+    lax.fori_loop(low, high, turn, 0)
 
 
 def kernel(
@@ -43,12 +82,6 @@
     def greet(d):
         pl.semaphore_signal(barrier, inc=1, device_id={"fs": d}, device_id_type=MESH)
 
-    each_partner(me, n_fs, greet)
-    for k in range(1, n_tp):
-        pl.semaphore_signal(
-            barrier, inc=1, device_id={"tp": (j + k) % n_tp}, device_id_type=MESH
-        )
-
     small = [(ids_ref, ids), (group_ref, group), (gap_ref, gap), (gain_ref, gain), (tokens_ref, tokens)]
     large = [(down_ref, down_f), (gate_ref, gate_f), (up_ref, up_f)]
     loads = [
@@ -57,6 +90,11 @@
     ]
     for c in loads:
         c.start()
+    far_partners_first(me, greet)
+    for k in range(1, n_tp):
+        pl.semaphore_signal(
+            barrier, inc=1, device_id={"tp": (j + k) % n_tp}, device_id_type=MESH
+        )
     for c in loads[:5]:
         c.wait()
 
@@ -95,15 +133,9 @@
         up_out[at] = (up_f[at] * scale).astype(BF16)
         return 0
 
-    loads[5].wait()
-    lax.fori_loop(0, n_fs // 8, round_down, 0)
-    loads[6].wait()
-    loads[7].wait()
-    lax.fori_loop(0, n_fs // 8, round_first, 0)
-
     pl.semaphore_wait(barrier, n_fs - 1 + n_tp - 1)
 
-    def exchange(i, src, dst):
+    def sender(i, src, dst):
         def send(d):
             pltpu.make_async_remote_copy(
                 src_ref=src.at[d], dst_ref=dst.at[me],
@@ -111,7 +143,10 @@
                 device_id={"fs": d}, device_id_type=MESH,
             ).start()
 
-        each_partner(me, n_fs, send)
+        return send
+
+    def exchange(i, src, dst):
+        each_partner(me, n_fs, sender(i, src, dst))
         dst[me] = src[me]
 
     def all_of(i, src, dst, copies=n_fs - 1):
@@ -122,15 +157,20 @@
         )
 
     exchange(0, tok_out, tok_in)
+    loads[5].wait()
+    lax.fori_loop(0, n_fs // 8, round_down, 0)
     exchange(1, down_out, down_in)
+    loads[6].wait()
+    loads[7].wait()
+    lax.fori_loop(0, n_fs // 8, round_first, 0)
     exchange(2, gate_out, gate_in)
     exchange(3, up_out, up_in)
 
     def across(i, src_of, dst):
-        for k in range(1, n_tp):
+        for k in (2, 1, 3):
             to = (j + k) % n_tp
             pltpu.make_async_remote_copy(
-                src_ref=src_of(to), dst_ref=dst.at[j],
+                src_ref=src_of(to), dst_ref=dst,
                 send_sem=send_sem.at[i], recv_sem=recv_sem.at[i],
                 device_id={"tp": to}, device_id_type=MESH,
             ).start()
@@ -139,10 +179,10 @@
     wide[...] = tok_in[...].reshape(slots * 4, 128).astype(F32)
     for b in range(4):
         rows_all[j, :, b * 128 : (b + 1) * 128] = wide[pl.ds(b, slots, stride=4), :].astype(BF16)
-    across(4, lambda to: rows_all.at[j], rows_all)
+    across(4, lambda to: rows_all.at[j], rows_all.at[j])
 
     all_of(1, down_out, down_in).wait_recv()
-    across(5, lambda to: down_in.at[pl.ds(to * (n_fs // n_tp), n_fs // n_tp)], down_q)
+    across(5, lambda to: down_in.at[pl.ds(to * (n_fs // n_tp), n_fs // n_tp)], down_q.at[j])
     down_q[j] = down_in[pl.ds(j * (n_fs // n_tp), n_fs // n_tp)]
 
     all_of(4, rows_all, rows_all, n_tp - 1).wait_recv()
@@ -160,21 +200,29 @@
     gate_acc = product(gate_in)
     all_of(3, up_out, up_in).wait_recv()
     up_acc = product(up_in)
-    hid_all[j] = (gate_acc / (1.0 + jnp.exp(-gate_acc)) * up_acc).astype(BF16)
-    across(6, lambda to: hid_all.at[j], hid_all)
+    hidden = (gate_acc / (1.0 + jnp.exp(-gate_acc)) * up_acc).astype(BF16)
+    for h in range(2):
+        hid_all[h, j] = hidden[h * n_fs : (h + 1) * n_fs]
+        across(6 + h, lambda to: hid_all.at[h, j], hid_all.at[h, j])
     all_of(5, down_q, down_q, n_tp - 1).wait_recv()
-    all_of(6, hid_all, hid_all, n_tp - 1).wait_recv()
-    total = None
-    for k in range(n_tp):
-        term = lax.dot_general(
-            hid_all[k], down_q[k].reshape(depth * 16, 128), (((1,), (1,)), ((), ())),
-            preferred_element_type=F32,
+
+    for h in range(2):
+        all_of(6 + h, hid_all.at[h], hid_all.at[h], n_tp - 1).wait_recv()
+        total = None
+        for k in range(n_tp):
+            term = lax.dot_general(
+                hid_all[h, k], down_q[k].reshape(depth * 16, 128), (((1,), (1,)), ((), ())),
+                preferred_element_type=F32,
+            )
+            total = term if total is None else total + term
+        for b in range(4):
+            wide[pl.ds(h * slots * 2 + b, n_fs, stride=4), :] = total[:, b * 128 : (b + 1) * 128]
+        half = pl.ds(h * n_fs // 2, n_fs // 2)
+        ret_out[half] = (
+            wide[h * slots * 2 : (h + 1) * slots * 2].astype(BF16).reshape(n_fs // 2, 8, 128)
         )
-        total = term if total is None else total + term
-    for b in range(4):
-        wide[pl.ds(b, slots, stride=4), :] = total[:, b * 128 : (b + 1) * 128]
-    ret_out[...] = wide[...].astype(BF16).reshape(n_fs, 8, 128)
-    exchange(7, ret_out, ret_in)
+        each_partner_of_rows(me, h * 4, h * 4 + 4, sender(8, ret_out, ret_in))
+    ret_in[me] = ret_out[me]
 
     here = lax.broadcasted_iota(jnp.int32, (count, count), 0) == lax.broadcasted_iota(
         jnp.int32, (count, count), 1
@@ -184,7 +232,7 @@
     w_first = jnp.sum(jnp.where(here, w_first, 0.0), axis=1, keepdims=True)
     w_second = jnp.sum(jnp.where(here, w_second, 0.0), axis=1, keepdims=True)
 
-    all_of(7, ret_out, ret_in).wait_recv()
+    all_of(8, ret_out, ret_in).wait_recv()
     wide[...] = ret_in[...].reshape(slots * 4, 128).astype(F32)
     for b in range(4):
         block = wide[pl.ds(b, slots, stride=4), :].astype(BF16)
@@ -202,9 +250,22 @@
         [(tok_out, tok_in), (down_out, down_in), (gate_out, gate_in), (up_out, up_in)]
     ):
         all_of(i, src, dst).wait_send()
-    for i, a in ((4, rows_all), (5, down_q), (6, hid_all)):
+    for i, a in ((4, rows_all), (5, down_q), (6, hid_all.at[0]), (7, hid_all.at[1])):
         all_of(i, a, a, n_tp - 1).wait_send()
-    all_of(7, ret_out, ret_in).wait_send()
+    all_of(8, ret_out, ret_in).wait_send()
+
+
+def place(gate_in, up_in, down_in, mixed_in, gate_ref, up_ref, down_ref, mixed_ref, sem):
+    copies = [
+        pltpu.make_async_copy(src, dst, sem.at[i])
+        for i, (src, dst) in enumerate(
+            [(gate_in, gate_ref), (up_in, up_ref), (down_in, down_ref), (mixed_in, mixed_ref)]
+        )
+    ]
+    for c in copies:
+        c.start()
+    for c in copies:
+        c.wait()
 
 
 def body(
@@ -214,12 +275,13 @@
     count, width = tokens.shape
     experts, depth, units = gate_weight.shape
     whole = pl.BlockSpec(memory_space=pltpu.VMEM)
-    anywhere = pl.BlockSpec(memory_space=pl.ANY)
+    anywhere = pl.BlockSpec(memory_space=pltpu.HBM)
     weights = jax.ShapeDtypeStruct((experts, depth, units), BF16)
     slots = 2 * n_fs
-    gate_new, up_new, down_new, mixed = pl.pallas_call(
+    results = (weights, weights, weights, jax.ShapeDtypeStruct((count, width), BF16))
+    held = pl.pallas_call(
         functools.partial(kernel, n_fs, n_tp),
-        out_shape=(weights, weights, weights, jax.ShapeDtypeStruct((count, width), BF16)),
+        out_shape=tuple(pltpu.VMEM(r.shape, r.dtype) for r in results),
         in_specs=[anywhere] * 8,
         out_specs=[whole] * 4,
         scratch_shapes=[
@@ -234,21 +296,29 @@
         + [pltpu.VMEM((n_fs, 8, 128), BF16)] * 4
         + [
             pltpu.VMEM((n_tp, slots, width), BF16),
-            pltpu.VMEM((n_tp, slots, units), BF16),
+            pltpu.VMEM((2, n_tp, n_fs, units), BF16),
             pltpu.VMEM((n_tp, n_fs // n_tp, depth, units), BF16),
             pltpu.VMEM((slots * 4, 128), F32),
             pltpu.VMEM((2, slots, count), BF16),
             pltpu.SemaphoreType.DMA((8,)),
-            pltpu.SemaphoreType.DMA((8,)),
-            pltpu.SemaphoreType.DMA((8,)),
+            pltpu.SemaphoreType.DMA((9,)),
+            pltpu.SemaphoreType.DMA((9,)),
         ],
         compiler_params=pltpu.CompilerParams(
-            collective_id=0, has_side_effects=True, vmem_limit_bytes=40 * 1024 * 1024
+            collective_id=0, has_side_effects=True, vmem_limit_bytes=65404928 - 8192
         ),
     )(
         route_ids.T, group_weight.reshape(1, count), logit_gap.reshape(1, count),
         norm_gain.reshape(1, depth), tokens, gate_weight, up_weight, down_weight,
     )
+    gate_new, up_new, down_new, mixed = pl.pallas_call(
+        place,
+        out_shape=results,
+        in_specs=[whole] * 4,
+        out_specs=[anywhere] * 4,
+        scratch_shapes=[pltpu.SemaphoreType.DMA((4,))],
+        compiler_params=pltpu.CompilerParams(vmem_limit_bytes=4 * 1024 * 1024),
+    )(*held)
     shape = (1, experts * depth, units)
     return gate_new.reshape(shape), up_new.reshape(shape), down_new.reshape(shape), mixed
 

time: 93.5 us -> 76.8 us (0.82)
  Pallas kernels: 84.3 us -> 76.1 us
  local copies, waits for them, and re-layouts: 8.2 us -> 0 us
    pallas_call x1 -> x2, Pallas kernels: 84.3 us -> 76.1 us  [the longest x1 74.9 us: body(): pl.pallas_call(functools.partial(kernel, n_fs, n_tp), out_shape=tuple((pl...]
    unnamed x20 -> x0, local copies, waits for them, and re-layouts: 8.2 us -> none
where the time goes in v2:
time: 76.8 us; the launch traced here: 76.7 us
  Pallas kernels  76.1 us (99%)
    pallas_call x1, Pallas kernels, body(): pl.pallas_call(functools.partial(kernel, n_fs, n_tp), out_shape=tuple((pl...  74.9 us

profile of v2, /device:TPU:1, one launch (start us, length us, event | category | flops | bytes accessed | tf_op | source)
XLA Modules:
  0.0 76.7 jit_solution(4006274802427516259)
XLA Ops:
  0.6 74.9 %shard_map.111 = (bf16[128,16,128]{2,1,0:T(8,128)(2,1)S(1)}, bf16[128,16,128]{2,1,0:T(8,128)(2,1)S(1)}, bf16[128,16,128]{2,1,0:T(8,128)(2,1)S(1)}, bf16[64,512]{1,0:T(8,128)(2,1)S(1)}) custom-call(s32[2,64]{1,0:T(2,128)} %bitcast.7, f32[1,64]{1,0:T(1,128)} %bitcast.8, f32[1,64]{1,0:T(1,128)} %bitcast.9, f32[1,16]{1,0:T(1,128)} %bitcast.10, ...), custom_call_target="tpu_custom_call" | custom-call | tf_op jit(solution)/shard_map/pallas_call | solution.py:282
  75.5 1.2 %shard_map.112 = (bf16[128,16,128]{2,1,0:T(8,128)(2,1)}, bf16[128,16,128]{2,1,0:T(8,128)(2,1)}, bf16[128,16,128]{2,1,0:T(8,128)(2,1)}, bf16[64,512]{1,0:T(8,128)(2,1)}) custom-call(bf16[128,16,128]{2,1,0:T(8,128)(2,1)S(1)} %get-tuple-element.12.gate_in, bf16[128,16,128]{2,1,0:T(8,128)(2,1)S(1)} %get-tuple-element.13.up_in, ...), custom_call_target="tpu_custom_call" | custom-call | tf_op jit(solution)/shard_map/pallas_call | solution.py:314

commit v3 on v2

--- a/solution.py
+++ b/solution.py
@@ -9,61 +9,69 @@
 
 MESH = pl.DeviceIdType.MESH
 F32, BF16 = jnp.float32, jnp.bfloat16
-STRIDE = 45
 FAR_FIRST = (4, 3, 5, 2, 6, 1, 7, 0)
-
-
-def partner(me, dz, dy, dc):
-    z, y, c = me // 16, (me // 2) % 8, me % 2
-    return ((z + dz) % 8) * 16 + ((y + dy) % 8) * 2 + (c + dc) % 2
-
-
-def each_partner(me, n_fs, step):
-    def at(n):
-        off = (n * STRIDE) % n_fs
-        step(partner(me, off // 16, (off // 2) % 8, off % 2))
-
-    def turn(i, _):
-        for u in range(8):
-            at(i * 8 + u)
-        return 0
-
-    for u in range(1, 8):
-        at(u)
-    lax.fori_loop(1, n_fs // 8, turn, 0)
-
-
-def far_partners_first(me, step):
-    def turn(k, _):
-        dz = (4 + (1 - 2 * (k % 2)) * ((k + 1) // 2)) % 8
-        for dy in FAR_FIRST:
-            for dc in range(2):
-                step(partner(me, dz, dy, dc))
-        return 0
-
-    lax.fori_loop(0, 7, turn, 0)
-    for dy in FAR_FIRST:
-        for dc in range(2):
-            if dy or dc:
-                step(partner(me, 0, dy, dc))
-
-
-def each_partner_of_rows(me, low, high, step):
-    z, y, c = me // 16, (me // 2) % 8, me % 2
-
-    def turn(row, _):
-        for dy in FAR_FIRST[:-1]:
-            for dc in range(2):
-                step(row * 16 + ((y + dy) % 8) * 2 + (c + dc) % 2)
-        step(row * 16 + y * 2 + (c + 1) % 2)
-
-        @pl.when(row != z)
+NEARING = sorted(
+    ((a, b) for a in range(8) for b in range(8)),
+    key=lambda t: -sum(min(FAR_FIRST[i], 8 - FAR_FIRST[i]) for i in t),
+)
+PIECES = 4
+
+
+class Torus:
+    def __init__(self, me):
+        self.z, y, self.c = me // 16, (me // 2) % 8, me % 2
+        self.places = [((y + dy) % 8) * 2 for dy in FAR_FIRST]
+        self.columns = [at + (self.c + dc) % 2 for at in self.places for dc in (1, 0)]
+        self.rows = tuple(((self.z + dz) % 8) * 16 for dz in FAR_FIRST)
+
+    def far_first(self, step):
+        def turn(_, rows):
+            for column in self.columns:
+                step(rows[0] + column)
+            return rows[1:] + rows[:1]
+
+        rows = lax.fori_loop(0, 7, turn, self.rows)
+        for column in self.columns[:-1]:
+            step(rows[0] + column)
+
+    def of_core_far_first(self, core, step):
+        for a, b in NEARING:
+            if a < 7 or b < 7:
+                step(self.rows[a] + self.places[b] + core)
+
+        @pl.when(self.c != core)
         def _():
-            step(row * 16 + y * 2 + c)
-
-        return 0
-
-    lax.fori_loop(low, high, turn, 0)
+            step(self.rows[7] + self.places[7] + core)
+
+    def of_core(self, core, step):
+        own, columns = self.c == core, [at + core for at in self.places]
+
+        def turn(_, rows):
+            for u, column in enumerate(columns):
+                step(rows[(3 * u + 2) % 8] + column)
+            return rows[1:] + rows[:1]
+
+        for u, column in enumerate(columns[:-1]):
+            step(self.rows[(3 * u + 2) % 8] + column)
+
+        @pl.when(jnp.logical_not(own))
+        def _():
+            step(self.rows[-1] + columns[-1])
+
+        lax.fori_loop(1, 8, turn, self.rows[1:] + self.rows[:1])
+
+    def row_by_row(self, low, high, step):
+        def turn(row, _):
+            for column in self.columns[:-1]:
+                step(row * 16 + column)
+
+            @pl.when(row != self.z)
+            def _():
+                step(row * 16 + self.columns[-1])
+
+            return 0
+
+        lax.fori_loop(low, high, turn, 0)
 
 
 def kernel(
@@ -77,6 +85,7 @@
 ):
     me, j = lax.axis_index("fs"), lax.axis_index("tp")
     slots = 2 * n_fs
+    torus = Torus(me)
     barrier = pltpu.get_barrier_semaphore()
 
     def greet(d):
@@ -90,7 +99,7 @@
     ]
     for c in loads:
         c.start()
-    far_partners_first(me, greet)
+    torus.far_first(greet)
     for k in range(1, n_tp):
         pl.semaphore_signal(
             barrier, inc=1, device_id={"tp": (j + k) % n_tp}, device_id_type=MESH
@@ -145,9 +154,8 @@
 
         return send
 
-    def exchange(i, src, dst):
-        each_partner(me, n_fs, sender(i, src, dst))
-        dst[me] = src[me]
+    def exchange(i, src, dst, core):
+        torus.of_core(core, sender(i, src, dst))
 
     def all_of(i, src, dst, copies=n_fs - 1):
         return pltpu.make_async_remote_copy(
@@ -156,15 +164,21 @@
             device_id={"tp": (j + 1) % n_tp}, device_id_type=MESH,
         )
 
-    exchange(0, tok_out, tok_in)
+    exchange(0, tok_out, tok_in, 0)
     loads[5].wait()
     lax.fori_loop(0, n_fs // 8, round_down, 0)
-    exchange(1, down_out, down_in)
+    exchange(1, down_out, down_in, 0)
     loads[6].wait()
     loads[7].wait()
     lax.fori_loop(0, n_fs // 8, round_first, 0)
-    exchange(2, gate_out, gate_in)
-    exchange(3, up_out, up_in)
+    exchange(2, gate_out, gate_in, 0)
+    torus.of_core_far_first(0, sender(3, up_out, up_in))
+    exchange(0, tok_out, tok_in, 1)
+    exchange(1, down_out, down_in, 1)
+    exchange(2, gate_out, gate_in, 1)
+    torus.of_core_far_first(1, sender(3, up_out, up_in))
+    for src, dst in ((tok_out, tok_in), (down_out, down_in), (gate_out, gate_in), (up_out, up_in)):
+        dst[me] = src[me]
 
     def across(i, src_of, dst):
         for k in (2, 1, 3):
@@ -201,12 +215,13 @@
     all_of(3, up_out, up_in).wait_recv()
     up_acc = product(up_in)
     hidden = (gate_acc / (1.0 + jnp.exp(-gate_acc)) * up_acc).astype(BF16)
-    for h in range(2):
-        hid_all[h, j] = hidden[h * n_fs : (h + 1) * n_fs]
+    per = slots // PIECES
+    for h in range(PIECES):
+        hid_all[h, j] = hidden[h * per : (h + 1) * per]
         across(6 + h, lambda to: hid_all.at[h, j], hid_all.at[h, j])
     all_of(5, down_q, down_q, n_tp - 1).wait_recv()
 
-    for h in range(2):
+    for h in range(PIECES):
         all_of(6 + h, hid_all.at[h], hid_all.at[h], n_tp - 1).wait_recv()
         total = None
         for k in range(n_tp):
@@ -216,12 +231,13 @@
             )
             total = term if total is None else total + term
         for b in range(4):
-            wide[pl.ds(h * slots * 2 + b, n_fs, stride=4), :] = total[:, b * 128 : (b + 1) * 128]
-        half = pl.ds(h * n_fs // 2, n_fs // 2)
-        ret_out[half] = (
-            wide[h * slots * 2 : (h + 1) * slots * 2].astype(BF16).reshape(n_fs // 2, 8, 128)
+            wide[pl.ds(h * per * 4 + b, per, stride=4), :] = total[:, b * 128 : (b + 1) * 128]
+        part = pl.ds(h * n_fs // PIECES, n_fs // PIECES)
+        ret_out[part] = (
+            wide[h * per * 4 : (h + 1) * per * 4].astype(BF16).reshape(n_fs // PIECES, 8, 128)
         )
-        each_partner_of_rows(me, h * 4, h * 4 + 4, sender(8, ret_out, ret_in))
+        rows = 8 // PIECES
+        torus.row_by_row(h * rows, (h + 1) * rows, sender(10, ret_out, ret_in))
     ret_in[me] = ret_out[me]
 
     here = lax.broadcasted_iota(jnp.int32, (count, count), 0) == lax.broadcasted_iota(
@@ -232,7 +248,7 @@
     w_first = jnp.sum(jnp.where(here, w_first, 0.0), axis=1, keepdims=True)
     w_second = jnp.sum(jnp.where(here, w_second, 0.0), axis=1, keepdims=True)
 
-    all_of(8, ret_out, ret_in).wait_recv()
+    all_of(10, ret_out, ret_in).wait_recv()
     wide[...] = ret_in[...].reshape(slots * 4, 128).astype(F32)
     for b in range(4):
         block = wide[pl.ds(b, slots, stride=4), :].astype(BF16)
@@ -250,9 +266,9 @@
         [(tok_out, tok_in), (down_out, down_in), (gate_out, gate_in), (up_out, up_in)]
     ):
         all_of(i, src, dst).wait_send()
-    for i, a in ((4, rows_all), (5, down_q), (6, hid_all.at[0]), (7, hid_all.at[1])):
+    for i, a in [(4, rows_all), (5, down_q)] + [(6 + h, hid_all.at[h]) for h in range(PIECES)]:
         all_of(i, a, a, n_tp - 1).wait_send()
-    all_of(8, ret_out, ret_in).wait_send()
+    all_of(10, ret_out, ret_in).wait_send()
 
 
 def place(gate_in, up_in, down_in, mixed_in, gate_ref, up_ref, down_ref, mixed_ref, sem):
@@ -296,13 +312,13 @@
         + [pltpu.VMEM((n_fs, 8, 128), BF16)] * 4
         + [
             pltpu.VMEM((n_tp, slots, width), BF16),
-            pltpu.VMEM((2, n_tp, n_fs, units), BF16),
+            pltpu.VMEM((PIECES, n_tp, slots // PIECES, units), BF16),
             pltpu.VMEM((n_tp, n_fs // n_tp, depth, units), BF16),
             pltpu.VMEM((slots * 4, 128), F32),
             pltpu.VMEM((2, slots, count), BF16),
             pltpu.SemaphoreType.DMA((8,)),
-            pltpu.SemaphoreType.DMA((9,)),
-            pltpu.SemaphoreType.DMA((9,)),
+            pltpu.SemaphoreType.DMA((7 + PIECES,)),
+            pltpu.SemaphoreType.DMA((7 + PIECES,)),
         ],
         compiler_params=pltpu.CompilerParams(
             collective_id=0, has_side_effects=True, vmem_limit_bytes=65404928 - 8192

time: 76.8 us -> 73.5 us (0.957)
  Pallas kernels: 76.1 us -> 72.7 us
    pallas_call x1, Pallas kernels: 74.9 us -> 71.5 us  [body(): pl.pallas_call(functools.partial(kernel, n_fs, n_tp), out_shape=tuple((pl...]
where the time goes in v3:
time: 73.5 us; the launch traced here: 73.3 us
  Pallas kernels  72.7 us (99%)
    pallas_call x1, Pallas kernels, body(): pl.pallas_call(functools.partial(kernel, n_fs, n_tp), out_shape=tuple((pl...  71.5 us

profile of v3, /device:TPU:1, one launch (start us, length us, event | category | flops | bytes accessed | tf_op | source)
XLA Modules:
  0.0 73.3 jit_solution(12515141193405392136)
XLA Ops:
  0.6 71.5 %shard_map.111 = (bf16[128,16,128]{2,1,0:T(8,128)(2,1)S(1)}, bf16[128,16,128]{2,1,0:T(8,128)(2,1)S(1)}, bf16[128,16,128]{2,1,0:T(8,128)(2,1)S(1)}, bf16[64,512]{1,0:T(8,128)(2,1)S(1)}) custom-call(s32[2,64]{1,0:T(2,128)} %bitcast.7, f32[1,64]{1,0:T(1,128)} %bitcast.8, f32[1,64]{1,0:T(1,128)} %bitcast.9, f32[1,16]{1,0:T(1,128)} %bitcast.10, ...), custom_call_target="tpu_custom_call" | custom-call | tf_op jit(solution)/shard_map/pallas_call | solution.py:298
  72.2 1.2 %shard_map.112 = (bf16[128,16,128]{2,1,0:T(8,128)(2,1)}, bf16[128,16,128]{2,1,0:T(8,128)(2,1)}, bf16[128,16,128]{2,1,0:T(8,128)(2,1)}, bf16[64,512]{1,0:T(8,128)(2,1)}) custom-call(bf16[128,16,128]{2,1,0:T(8,128)(2,1)S(1)} %get-tuple-element.12.gate_in, bf16[128,16,128]{2,1,0:T(8,128)(2,1)S(1)} %get-tuple-element.13.up_in, ...), custom_call_target="tpu_custom_call" | custom-call | tf_op jit(solution)/shard_map/pallas_call | solution.py:330

commit v4 on v3

--- a/solution.py
+++ b/solution.py
@@ -77,10 +77,10 @@
 def kernel(
     n_fs, n_tp,
     ids_ref, group_ref, gap_ref, gain_ref, tokens_ref, gate_ref, up_ref, down_ref,
-    gate_in, up_in, down_in, mixed_ref,
+    gate_in, up_in, down_in, ret_in, picks, shares,
     ids, group, gap, gain, tokens, gate_f, up_f, down_f,
-    gate_out, up_out, down_out, tok_out, tok_in, ret_out, ret_in,
-    rows_all, hid_all, down_q, wide, picks,
+    gate_out, up_out, down_out, tok_out, tok_in, ret_out,
+    rows_all, hid_all, down_q, wide,
     local_sem, send_sem, recv_sem,
 ):
     me, j = lax.axis_index("fs"), lax.axis_index("tp")
@@ -245,10 +245,29 @@
     )
     w_first = group[...] * jax.nn.sigmoid(gap[...])
     w_second = group[...] * jax.nn.sigmoid(-gap[...])
-    w_first = jnp.sum(jnp.where(here, w_first, 0.0), axis=1, keepdims=True)
-    w_second = jnp.sum(jnp.where(here, w_second, 0.0), axis=1, keepdims=True)
+    for k, w in enumerate((w_first, w_second)):
+        w = jnp.sum(jnp.where(here, w, 0.0), axis=1, keepdims=True)
+        shares[k] = jnp.broadcast_to(w, (count, 128))
 
     all_of(10, ret_out, ret_in).wait_recv()
+    for i, (src, dst) in enumerate(
+        [(tok_out, tok_in), (down_out, down_in), (gate_out, gate_in), (up_out, up_in)]
+    ):
+        all_of(i, src, dst).wait_send()
+    for i, a in [(4, rows_all), (5, down_q)] + [(6 + h, hid_all.at[h]) for h in range(PIECES)]:
+        all_of(i, a, a, n_tp - 1).wait_send()
+    all_of(10, ret_out, ret_in).wait_send()
+
+
+def finish(
+    gate_in, up_in, down_in, ret_in, picks, shares,
+    gate_ref, up_ref, down_ref, mixed_ref, wide, mixed, sem,
+):
+    pairs = [(gate_in, gate_ref), (up_in, up_ref), (down_in, down_ref), (mixed, mixed_ref)]
+    copies = [pltpu.make_async_copy(src, dst, sem.at[i]) for i, (src, dst) in enumerate(pairs)]
+    for c in copies[:3]:
+        c.start()
+    slots = picks.shape[1]
     wide[...] = ret_in[...].reshape(slots * 4, 128).astype(F32)
     for b in range(4):
         block = wide[pl.ds(b, slots, stride=4), :].astype(BF16)
@@ -258,28 +277,10 @@
             )
             for k in range(2)
         ]
-        mixed_ref[:, b * 128 : (b + 1) * 128] = (
-            w_first * value[0] + w_second * value[1]
+        mixed[:, b * 128 : (b + 1) * 128] = (
+            shares[0] * value[0] + shares[1] * value[1]
         ).astype(BF16)
-
-    for i, (src, dst) in enumerate(
-        [(tok_out, tok_in), (down_out, down_in), (gate_out, gate_in), (up_out, up_in)]
-    ):
-        all_of(i, src, dst).wait_send()
-    for i, a in [(4, rows_all), (5, down_q)] + [(6 + h, hid_all.at[h]) for h in range(PIECES)]:
-        all_of(i, a, a, n_tp - 1).wait_send()
-    all_of(10, ret_out, ret_in).wait_send()
-
-
-def place(gate_in, up_in, down_in, mixed_in, gate_ref, up_ref, down_ref, mixed_ref, sem):
-    copies = [
-        pltpu.make_async_copy(src, dst, sem.at[i])
-        for i, (src, dst) in enumerate(
-            [(gate_in, gate_ref), (up_in, up_ref), (down_in, down_ref), (mixed_in, mixed_ref)]
-        )
-    ]
-    for c in copies:
-        c.start()
+    copies[3].start()
     for c in copies:
         c.wait()
 
@@ -297,9 +298,14 @@
     results = (weights, weights, weights, jax.ShapeDtypeStruct((count, width), BF16))
     held = pl.pallas_call(
         functools.partial(kernel, n_fs, n_tp),
-        out_shape=tuple(pltpu.VMEM(r.shape, r.dtype) for r in results),
+        out_shape=(
+            *(pltpu.VMEM(r.shape, r.dtype) for r in results[:3]),
+            pltpu.VMEM((n_fs, 8, 128), BF16),
+            pltpu.VMEM((2, slots, count), BF16),
+            pltpu.VMEM((2, count, 128), F32),
+        ),
         in_specs=[anywhere] * 8,
-        out_specs=[whole] * 4,
+        out_specs=[whole] * 6,
         scratch_shapes=[
             pltpu.VMEM((2, count), jnp.int32),
             pltpu.VMEM((1, count), F32),
@@ -309,30 +315,33 @@
         ]
         + [pltpu.VMEM((experts, depth, units), F32)] * 3
         + [pltpu.VMEM((experts, depth, units), BF16)] * 3
-        + [pltpu.VMEM((n_fs, 8, 128), BF16)] * 4
+        + [pltpu.VMEM((n_fs, 8, 128), BF16)] * 3
         + [
             pltpu.VMEM((n_tp, slots, width), BF16),
             pltpu.VMEM((PIECES, n_tp, slots // PIECES, units), BF16),
             pltpu.VMEM((n_tp, n_fs // n_tp, depth, units), BF16),
             pltpu.VMEM((slots * 4, 128), F32),
-            pltpu.VMEM((2, slots, count), BF16),
             pltpu.SemaphoreType.DMA((8,)),
             pltpu.SemaphoreType.DMA((7 + PIECES,)),
             pltpu.SemaphoreType.DMA((7 + PIECES,)),
         ],
         compiler_params=pltpu.CompilerParams(
-            collective_id=0, has_side_effects=True, vmem_limit_bytes=65404928 - 8192
+            collective_id=0, has_side_effects=True, vmem_limit_bytes=67043328 - 1572864 - 262144 - 131072 - 65536 - 8192
         ),
     )(
         route_ids.T, group_weight.reshape(1, count), logit_gap.reshape(1, count),
         norm_gain.reshape(1, depth), tokens, gate_weight, up_weight, down_weight,
     )
     gate_new, up_new, down_new, mixed = pl.pallas_call(
-        place,
+        finish,
         out_shape=results,
-        in_specs=[whole] * 4,
+        in_specs=[whole] * 6,
         out_specs=[anywhere] * 4,
-        scratch_shapes=[pltpu.SemaphoreType.DMA((4,))],
+        scratch_shapes=[
+            pltpu.VMEM((slots * 4, 128), F32),
+            pltpu.VMEM((count, width), BF16),
+            pltpu.SemaphoreType.DMA((4,)),
+        ],
         compiler_params=pltpu.CompilerParams(vmem_limit_bytes=4 * 1024 * 1024),
     )(*held)
     shape = (1, experts * depth, units)

time: 73.5 us -> 73.1 us (level)
  no operation moved by 1% of the time
where the time goes in v4:
time: 73.1 us; the launch traced here: 73 us
  Pallas kernels  72.4 us (99%)
    pallas_call x1, Pallas kernels, body(): pl.pallas_call(functools.partial(kernel, n_fs, n_tp), out_shape=(*(pltpu....  71.2 us

profile of v4, /device:TPU:1, one launch (start us, length us, event | category | flops | bytes accessed | tf_op | source)
XLA Modules:
  0.0 73.0 jit_solution(13379129182716124580)
XLA Ops:
  0.6 71.2 %shard_map.111 = (bf16[128,16,128]{2,1,0:T(8,128)(2,1)S(1)}, bf16[128,16,128]{2,1,0:T(8,128)(2,1)S(1)}, bf16[128,16,128]{2,1,0:T(8,128)(2,1)S(1)}, bf16[128,8,12...) custom-call(s32[2,64]{1,0:T(2,128)} %bitcast.7, f32[1,64]{1,0:T(1,128)} %bitcast.8, ...), custom_call_target="tpu_custom_call" | custom-call | tf_op jit(solution)/shard_map/pallas_call | solution.py:299
  71.8 1.2 %shard_map.112 = (bf16[128,16,128]{2,1,0:T(8,128)(2,1)}, bf16[128,16,128]{2,1,0:T(8,128)(2,1)}, bf16[128,16,128]{2,1,0:T(8,128)(2,1)}, bf16[64,512]{1,0:T(8,128)(2,1)}) custom-call(bf16[128,16,128]{2,1,0:T(8,128)(2,1)S(1)} %get-tuple-element.14.gate_in, bf16[128,16,128]{2,1,0:T(8,128)(2,1)S(1)} %get-tuple-element.15.up_in, ...), custom_call_target="tpu_custom_call" | custom-call | tf_op jit(solution)/shard_map/pallas_call | solution.py:335
